TPU v7x, 512 devices: a whole 4x8x8 slice. The times are simulated.
512 devices in a mesh: ep: 32 (over z, x), tp: 16 (over y, core).
Axes of the slice: x: 4, y: 8, z: 8, core: 2. Of those that a mesh axis runs over, the one named last changes fastest.
Arguments:
- tokens: bfloat16 [8192, 2048], P('ep')
- norm_gain: float32 [2048], replicated, may hold values from 0.1 to 1.9
- chosen: int32 [32, 1024], replicated, may hold values from 0 to 8191, as said below
- route_weight: float32 [32, 1024], P('ep'), may hold values from 0.2 to 1
- gate_weight: bfloat16 [32, 2048, 4096], P('ep', None, 'tp'), may hold values from -0.125 to 0.125
- up_weight: bfloat16 [32, 2048, 4096], P('ep', None, 'tp'), may hold values from -0.125 to 0.125
- down_weight: bfloat16 [32, 4096, 2048], P('ep', 'tp'), may hold values from -0.09375 to 0.09375
Outputs:
- combined: bfloat16 [8192, 2048], P('ep', 'tp')
Inputs may be any that keep to these rules, and one draw needn't show every extreme that they name: Each row of chosen lists 1024 distinct token numbers in ascending order. Of the 256 consecutive tokens of one index of ep, a row holds at most 48, and every draw has rows that hold exactly 48 of them.
All inputs are finite; a program needn't handle non-finite values.
Results may differ from a plain program's by a relative error of at most 0.02.
Values may be sent and summed in bfloat16 or wider, within the bound.
No kernel may reach another device: no remote copies, remote signals or barrier semaphores. Data moves between devices by JAX's collectives and lax.ppermute only.
A program may use at most 64 MiB of HBM per device.

v0:
```python
import jax
import jax.numpy as jnp
from jax import lax
from jax.sharding import Mesh
from jax.sharding import PartitionSpec as P

EP = ("ep_0", "ep_1")


def whole_of(x, axes, dim):
    if not axes:
        return x
    nearer = lax.all_gather(x, axes[-1], axis=dim, tiled=True)
    return whole_of(nearer, axes[:-1], dim)


def shards(tokens, norm_gain, chosen, route_weight, gate_weight, up_weight, down_weight):
    tok_rows, row_width = tokens.shape
    experts, capacity = chosen.shape
    ep_count = lax.axis_size(EP)
    tp_count = lax.axis_size("tp")
    owner_index = lax.axis_index(EP)
    lane_index = lax.axis_index("tp")
    slot_most = 3 * tok_rows // 16
    col_width = row_width // tp_count
    values = tokens.astype(jnp.float32)
    scale = lax.rsqrt(jnp.mean(values * values, axis=-1, keepdims=True) + 1e-06)
    normed = (values * scale * norm_gain[None, :]).astype(jnp.bfloat16)
    slot_steps = jnp.arange(slot_most, dtype=jnp.int32)
    first_token = owner_index * tok_rows
    run_start = jnp.sum((chosen < first_token).astype(jnp.int32), axis=1)
    run_end = jnp.sum((chosen < first_token + tok_rows).astype(jnp.int32), axis=1)
    run_count = run_end - run_start
    slot_live = slot_steps[None, :] < run_count[:, None]
    slot_place = jnp.minimum(run_start[:, None] + slot_steps[None, :], capacity - 1)
    slot_token = jnp.take_along_axis(chosen, slot_place, axis=1) - first_token
    my_chosen = lax.dynamic_index_in_dim(chosen, owner_index, 0, keepdims=False)
    block_edges = jnp.arange(ep_count, dtype=jnp.int32) * tok_rows
    src_start = jnp.sum((my_chosen[None, :] < block_edges[:, None]).astype(jnp.int32), axis=1)
    src_end = jnp.concatenate([src_start[1:], jnp.full((1,), capacity, jnp.int32)])
    gate_mat = gate_weight[0]
    up_mat = up_weight[0]
    down_mat = down_weight[0]
    my_columns = lax.dynamic_slice_in_dim(normed, lane_index * col_width, col_width, 1)
    all_columns = whole_of(my_columns, EP, 0)
    picked_rows = all_columns[my_chosen]
    segment = lax.all_gather(picked_rows, "tp", axis=1, tiled=True)
    gate_pre = jnp.dot(segment, gate_mat, preferred_element_type=jnp.float32)
    up_pre = jnp.dot(segment, up_mat, preferred_element_type=jnp.float32)
    hidden = (jax.nn.silu(gate_pre) * up_pre).astype(jnp.bfloat16)
    summed_out = lax.psum_scatter(
        lax.dot_general(
            down_mat, hidden, (((0,), (1,)), ((), ())), preferred_element_type=jnp.float32
        ).astype(jnp.bfloat16),
        "tp",
        scatter_dimension=0,
        tiled=True,
    ).astype(jnp.float32)
    weighted = (summed_out.T * route_weight[0][:, None]).astype(jnp.bfloat16)
    back_place = jnp.minimum(src_start[:, None] + slot_steps[None, :], capacity - 1)
    back_live = slot_steps[None, :] < (src_end - src_start)[:, None]
    outgoing_back = jnp.where(
        back_live[:, :, None], weighted[back_place], jnp.zeros((), jnp.bfloat16)
    )
    returned = lax.all_to_all(outgoing_back, EP, split_axis=0, concat_axis=0, tiled=True)
    target_row = jnp.where(slot_live, slot_token, tok_rows).reshape(-1)
    placement = (jnp.arange(tok_rows, dtype=jnp.int32)[:, None] == target_row[None, :]).astype(
        jnp.bfloat16
    )
    combined = jnp.dot(
        placement, returned.reshape(-1, col_width), preferred_element_type=jnp.float32
    )
    return combined.astype(jnp.bfloat16)


def solution(mesh):
    finer = Mesh(mesh.devices.reshape(8, 4, mesh.shape["tp"]), ("ep_0", "ep_1", "tp"))
    in_specs = (
        P(EP, None),
        P(),
        P(),
        P(EP, None),
        P(EP, None, "tp"),
        P(EP, None, "tp"),
        P(EP, "tp", None),
    )
    out_specs = P(EP, "tp")
    return jax.shard_map(
        shards, mesh=finer, in_specs=in_specs, out_specs=out_specs, check_vma=False
    )
```

profile of v0, /device:TPU:2, one launch (start us, length us, event | category | flops | bytes accessed | tf_op | source)
XLA Modules:
  0.0 248.7 jit_solution(2484285183497416496)
XLA Ops:
  6.5 1.5 convert_element_type.40
  8.1 1.5 multiply_reduce_fusion
  9.6 0.8 dynamic-slice
  10.4 0.1 fusion.17
  10.5 15.7 %all_gather.9 = bf16[1024,128]{1,0:T(8,128)(2,1)} all-gather(bf16[256,128]{1,0:T(8,128)(2,1)S(1)} %fusion.17), channel_id=1, replica_groups=mesh['ep_0'=8,'ep_1'=4,'tp'=16] {'ep_1'}, dimensions={0}, use_global_device_ids=true | all-gather | bytes 327680 | tf_op jit(solution)/shard_map/all_gather | solution.py:13
  26.3 46.0 %all-gather.4.cloned.1.call-done = bf16[8192,128]{1,0:T(8,128)(2,1)} async-done(((bf16[1024,128]{1,0:T(8,128)(2,1)}), bf16[8192,128]{1,0:T(8,128)(2,1)}) %all-gather.4.cloned.1.call-update) | async-done | bytes 2097168 | tf_op jit(solution)/shard_map/all_gather | solution.py:13
  72.3 5.9 %gather_fusion = bf16[1024,128]{1,0:T(8,128)(2,1)} fusion(bf16[8192,128]{1,0:T(8,128)(2,1)} %all-gather.4.cloned.1.call-done, s32[1024]{0:T(1024)S(1)} %broadcast_clamp_fusion), kind=kCustom, calls=%fused_computation | custom fusion | bytes 528384 | tf_op jit(solution)/shard_map/gather | solution.py:46
  78.3 49.9 %all-gather.6.cloned.1.call-done = bf16[1024,2048]{1,0:T(8,128)(2,1)} async-done(((bf16[1024,128]{1,0:T(8,128)(2,1)}), bf16[1024,2048]{1,0:T(8,128)(2,1)}) %all-gather.6.cloned.1.call-update) | async-done | bytes 4194320 | tf_op jit(solution)/shard_map/all_gather | solution.py:47
  128.2 3.7 %fusion.6 = f32[1024,256]{1,0:T(8,128)S(1)} fusion(bf16[1024,2048]{1,0:T(8,128)(2,1)} %all-gather.6.cloned.1.call-done, bf16[1,2048,256]{2,1,0:T(8,128)(2,1)} %param.11), kind=kOutput, calls=%fused_computation.12 | convolution fusion | flops 1073741824 | bytes 6291456 | tf_op jit(solution)/shard_map/dot_general | solution.py:48
  132.0 8.5 %convert_bitcast_fusion = bf16[2048,1024]{0,1:T(8,128)(2,1)} fusion(bf16[1024,2048]{1,0:T(8,128)(2,1)} %all-gather.6.cloned.1.call-done, bf16[1,256,2048]{2,1,0:T(8,128)(2,1)S(1)} %copy-done, bf16[1,2048,256]{2,1,0:T(8,128)(2,1)S(1)} %copy-done.3, f32[1024,256]{1,0:T(8,128)S(1)} %fusion.6), kind=kOutput, calls=%fused_computation.3 | convolution fusion | flops 2151153664 | bytes 11534336 | tf_op jit(solution)/shard_map/dot_general | solution.py:52
  140.5 6.4 %copy.8 = bf16[2048,1024]{1,0:T(8,128)(2,1)} copy(bf16[2048,1024]{0,1:T(8,128)(2,1)} %convert_bitcast_fusion) | data formatting | bytes 8388608
  146.9 0.2 convert_reduce_fusion
  147.1 0.1 slice.3
  147.2 0.1 compare_select_fusion
  147.3 0.1 reshape.234
  147.4 0.1 add_subtract_fusion
  147.4 0.1 iota_compare_fusion.4
  147.5 64.2 %reduce-scatter.4.cloned.1.call-done = bf16[128,1024]{1,0:T(8,128)(2,1)} async-done(((bf16[2048,1024]{1,0:T(8,128)(2,1)}), bf16[128,1024]{1,0:T(8,128)(2,1)}) %reduce-scatter.4.cloned.1.call-update) | async-done | bytes 262160
  211.7 1.1 copy.9
  212.8 0.2 fusion.15
  213.0 3.2 %gather_fusion.1 = bf16[1536,128]{1,0:T(8,128)(2,1)S(1)} fusion(bf16[1024,128]{1,0:T(8,128)(2,1)S(1)} %fusion.15, s32[2048]{0:T(1024)S(1)} %pad_clamp_fusion), kind=kCustom, calls=%fused_computation.1 | custom fusion | bytes 792576 | tf_op jit(solution)/shard_map/gather | solution.py:63
  216.2 1.0 broadcast_select_fusion
  217.3 10.5 %all-to-all-start = ((bf16[32,48,128]{2,1,0:T(8,128)(2,1)}), bf16[32,48,128]{2,1,0:T(8,128)(2,1)S(1)}, u32[]{:S(2)}, u32[]{:S(2)}) async-start(bf16[32,48,128]{2,1,0:T(8,128)(2,1)} %broadcast_select_fusion), calls=%async_computation | async-start | bytes 786432 | tf_op jit(solution)/shard_map/all_to_all | solution.py:65
  227.8 0.1 convert_reduce_fusion.1
  227.9 0.1 iota_compare_fusion.5
  228.0 0.1 lt.135
  228.1 0.1 fusion.20
  228.2 0.1 reshape.240
  228.2 12.6 %gather_fusion.2 = s32[1536]{0:T(1024)S(1)} fusion(s32[32,1024]{1,0:T(8,128)S(1)} %copy-done.1, s32[1536]{0:T(1024)S(1)} %reshape.240), kind=kCustom, calls=%fused_computation.2 | custom fusion | bytes 24576 | tf_op jit(solution)/shard_map/jit(take_along_axis)/gather | solution.py:36
  240.9 0.1 add.130
  241.0 0.1 lt.137
  241.1 1.0 fusion.2
  (24 shorter events, 0.3 us)
Async XLA Ops:
  6.5 125.4 %copy-start = (bf16[1,256,2048]{2,1,0:T(8,128)(2,1)S(1)}, bf16[1,256,2048]{2,1,0:T(8,128)(2,1)}, u32[]{:S(2)}) copy-start(bf16[1,256,2048]{2,1,0:T(8,128)(2,1)} %param.13) | copy-start | bytes 3145732
  6.5 19.7 %copy-start.1 = (s32[32,1024]{1,0:T(8,128)S(1)}, s32[32,1024]{1,0:T(8,128)}, u32[]{:S(2)}) copy-start(s32[32,1024]{1,0:T(8,128)} %param.9) | copy-start | bytes 393220
  6.5 65.7 %all-gather.4.cloned.1.call-start = ((), (), s32[]{:S(2)}) async-start(), calls=%async_computation.2 | async-start | bytes 2359296 | tf_op jit(solution)/shard_map/all_gather | solution.py:13
  26.2 102.0 %all-gather.6.cloned.1.call-start = ((), (), s32[]{:S(2)}) async-start(), calls=%async_computation.3 | async-start | bytes 4456448 | tf_op jit(solution)/shard_map/all_gather | solution.py:47
  78.2 53.8 %copy-start.3 = (bf16[1,2048,256]{2,1,0:T(8,128)(2,1)S(1)}, bf16[1,2048,256]{2,1,0:T(8,128)(2,1)}, u32[]{:S(2)}) copy-start(bf16[1,2048,256]{2,1,0:T(8,128)(2,1)} %param.12) | copy-start | bytes 3145732
  78.2 133.5 %reduce-scatter.4.cloned.1.call-start = ((), (), s32[]{:S(2)}) async-start(), calls=%async_computation.4 | async-start | bytes 4456448
  146.9 65.9 %copy-start.2 = (f32[1,1024]{1,0:T(1,128)S(1)}, f32[1,1024]{1,0:T(1,128)}, u32[]{:S(2)}) copy-start(f32[1,1024]{1,0:T(1,128)} %param.10) | copy-start | bytes 12292
  217.3 23.9 %all-to-all-start = ((bf16[32,48,128]{2,1,0:T(8,128)(2,1)}), bf16[32,48,128]{2,1,0:T(8,128)(2,1)S(1)}, u32[]{:S(2)}, u32[]{:S(2)}) async-start(bf16[32,48,128]{2,1,0:T(8,128)(2,1)} %broadcast_select_fusion), calls=%async_computation | async-start | bytes 786432 | tf_op jit(solution)/shard_map/all_to_all | solution.py:65
Sparse Core Ops, SparseCore 0:
  26.3 45.9 all-gather.3
  78.3 49.8 all-gather.5
  147.0 64.5 reduce-scatter.3
where the time goes:
time: 249 us
  waiting for transfers between devices  160 us (64%)
  local copies, waits for them, and re-layouts  30.6 us (12%)
  blocking collectives  15.7 us (6%)
  matrix products  13.3 us (5%)
  between operations  13.3 us (5%)
  starting transfers between devices  10.6 us (4%)
  other arithmetic  5.16 us (2%)
    unnamed x4, waiting for transfers between devices  64.2 us
    all_gather x1, waiting for transfers between devices, shards(): segment = lax.all_gather(picked_rows, 'tp', axis=1, tiled=True)  49.9 us
    all_gather x1, waiting for transfers between devices, whole_of(): nearer = lax.all_gather(x, axes[-1], axis=dim, tiled=True)  46 us
    all_gather x1, blocking collectives, whole_of(): nearer = lax.all_gather(x, axes[-1], axis=dim, tiled=True)  15.7 us
    gather x2, local copies, waits for them, and re-layouts, shards(): slot_token = jnp.take_along_axis(chosen, slot_place, axis=1) - first_token  12.7 us
    all_to_all x1, starting transfers between devices, shards(): lax.all_to_all(outgoing_back, EP, split_axis=0, concat_axis=0, tiled=True)  10.5 us
    dot_general x1, matrix products, shards(): lax.dot_general(down_mat, hidden, (((0,), (1,)), ((), ())), preferred_ele...  8.52 us
    unnamed x10, local copies, waits for them, and re-layouts  7.53 us
  transfers between devices with their start and end apart: 4, of which 3 were waited for; matrix products, arithmetic and copies ran while one was open for 6% of the time, Pallas kernels for 0%

commit v1 on v0

--- a/solution.py
+++ b/solution.py
@@ -44,7 +44,8 @@
     my_columns = lax.dynamic_slice_in_dim(normed, lane_index * col_width, col_width, 1)
     all_columns = whole_of(my_columns, EP, 0)
     picked_rows = all_columns[my_chosen]
-    segment = lax.all_gather(picked_rows, "tp", axis=1, tiled=True)
+    sent = jnp.stack([picked_rows] * lax.axis_size("tp"))
+    segment = jnp.concatenate(lax.all_to_all(sent, "tp", 0, 0), axis=1)
     gate_pre = jnp.dot(segment, gate_mat, preferred_element_type=jnp.float32)
     up_pre = jnp.dot(segment, up_mat, preferred_element_type=jnp.float32)
     hidden = (jax.nn.silu(gate_pre) * up_pre).astype(jnp.bfloat16)

time: 249 us -> 298 us (1.20)
  blocking collectives: 15.7 us -> 117 us
  waiting for transfers between devices: 160 us -> 107 us
    all_to_all x0 -> x1, blocking collectives: none -> 101 us  [shards(): segment = jnp.concatenate(lax.all_to_all(sent, 'tp', 0, 0), axis=1)]
    all_gather x1 -> x0, waiting for transfers between devices: 49.9 us -> none  [shards(): segment = lax.all_gather(picked_rows, 'tp', axis=1, tiled=True)]
    unnamed x4 -> x3, waiting for transfers between devices: 64.2 us -> 61 us
    unnamed x10 -> x14, local copies, waits for them, and re-layouts: 7.53 us -> 9.51 us
  transfers between devices with their start and end apart: 4 -> 3, of which waited for: 3 -> 2; matrix products, arithmetic and copies ran while one was open for 6% -> 5% of each run, Pallas kernels for 0% -> 0%
where the time goes in v1:
time: 298 us; the launch traced here: 297 us
  blocking collectives  117 us (39%)
  waiting for transfers between devices  107 us (36%)
  local copies, waits for them, and re-layouts  32 us (11%)
  between operations  13.6 us (5%)
  matrix products  12.1 us (4%)
  starting transfers between devices  10.6 us (4%)
  other arithmetic  5.15 us (2%)
    all_to_all x1, blocking collectives, shards(): segment = jnp.concatenate(lax.all_to_all(sent, 'tp', 0, 0), axis=1)  101 us
    unnamed x3, waiting for transfers between devices  61 us
    all_gather x1, waiting for transfers between devices, whole_of(): nearer = lax.all_gather(x, axes[-1], axis=dim, tiled=True)  46 us
    all_gather x1, blocking collectives, whole_of(): nearer = lax.all_gather(x, axes[-1], axis=dim, tiled=True)  15.7 us
    gather x2, local copies, waits for them, and re-layouts, shards(): slot_token = jnp.take_along_axis(chosen, slot_place, axis=1) - first_token  12.7 us
    all_to_all x1, starting transfers between devices, shards(): lax.all_to_all(outgoing_back, EP, split_axis=0, concat_axis=0, tiled=True)  10.5 us
    unnamed x14, local copies, waits for them, and re-layouts  9.51 us
    dot_general x1, matrix products, shards(): lax.dot_general(down_mat, hidden, (((0,), (1,)), ((), ())), preferred_ele...  8.8 us
  transfers between devices with their start and end apart: 3, of which 2 were waited for; matrix products, arithmetic and copies ran while one was open for 5% of the time, Pallas kernels for 0%

profile of v1, /device:TPU:2, one launch (start us, length us, event | category | flops | bytes accessed | tf_op | source)
XLA Modules:
  0.0 297.5 jit_solution(8169380558942679593)
XLA Ops:
  6.5 1.5 convert_element_type.40
  8.1 1.5 multiply_reduce_fusion
  9.6 0.8 dynamic-slice
  10.4 0.1 fusion.17
  10.5 15.7 %all_gather.6 = bf16[1024,128]{1,0:T(8,128)(2,1)} all-gather(bf16[256,128]{1,0:T(8,128)(2,1)S(1)} %fusion.17), channel_id=1, replica_groups=mesh['ep_0'=8,'ep_1'=4,'tp'=16] {'ep_1'}, dimensions={0}, use_global_device_ids=true | all-gather | bytes 327680 | tf_op jit(solution)/shard_map/all_gather | solution.py:13
  26.3 46.0 %all-gather.2.cloned.1.call-done = bf16[8192,128]{1,0:T(8,128)(2,1)} async-done(((bf16[1024,128]{1,0:T(8,128)(2,1)}), bf16[8192,128]{1,0:T(8,128)(2,1)}) %all-gather.2.cloned.1.call-update) | async-done | bytes 2097168 | tf_op jit(solution)/shard_map/all_gather | solution.py:13
  72.3 4.7 %gather_fusion = bf16[1024,128]{1,0:T(8,128)(2,1)S(1)} fusion(bf16[8192,128]{1,0:T(8,128)(2,1)} %all-gather.2.cloned.1.call-done, s32[1024]{0:T(1024)S(1)} %broadcast_clamp_fusion), kind=kCustom, calls=%fused_computation | custom fusion | bytes 528384 | tf_op jit(solution)/shard_map/gather | solution.py:46
  77.0 0.1 copy.10
  77.2 0.5 stack.2
  77.7 101.4 %all_to_all.10 = bf16[16,1024,128]{1,2,0:T(8,128)(2,1)S(1)} all-to-all(bf16[16,1024,128]{1,2,0:T(8,128)(2,1)S(1)} %stack.2), channel_id=1, replica_groups=mesh['ep_0'=8,'ep_1'=4,'tp'=16] {'tp'}, dimensions={0} | all-to-all | bytes 8388608 | tf_op jit(solution)/shard_map/all_to_all | solution.py:48
  179.1 2.0 copy-done.2
  181.0 2.3 fusion.6
  183.4 8.8 %convert_bitcast_fusion = bf16[2048,1024]{0,1:T(8,128)(2,1)} fusion(bf16[1024,2048]{0,1:T(8,128)(2,1)} %bitcast.37, bf16[1,256,2048]{2,1,0:T(8,128)(2,1)S(1)} %copy-done, bf16[1,2048,256]{2,1,0:T(8,128)(2,1)S(1)} %copy-done.5, f32[1024,256]{1,0:T(8,128)} %fusion.6), kind=kOutput, calls=%fused_computation.3 | convolution fusion | flops 2151153664 | bytes 11534336 | tf_op jit(solution)/shard_map/dot_general | solution.py:53
  192.2 6.4 %copy.11 = bf16[2048,1024]{1,0:T(8,128)(2,1)} copy(bf16[2048,1024]{0,1:T(8,128)(2,1)} %convert_bitcast_fusion) | data formatting | bytes 8388608
  198.6 0.2 convert_reduce_fusion
  198.8 0.1 slice.3
  198.9 0.1 compare_select_fusion
  199.0 0.1 reshape.244
  199.1 0.1 add_subtract_fusion
  199.1 0.1 iota_compare_fusion.4
  199.2 61.0 %reduce-scatter.4.cloned.1.call-done = bf16[128,1024]{1,0:T(8,128)(2,1)} async-done(((bf16[2048,1024]{1,0:T(8,128)(2,1)}), bf16[128,1024]{1,0:T(8,128)(2,1)}) %reduce-scatter.4.cloned.1.call-update) | async-done | bytes 262160
  260.2 1.1 copy.12
  261.3 0.2 fusion.15
  261.5 3.2 %gather_fusion.1 = bf16[1536,128]{1,0:T(8,128)(2,1)S(1)} fusion(bf16[1024,128]{1,0:T(8,128)(2,1)S(1)} %fusion.15, s32[2048]{0:T(1024)S(1)} %pad_clamp_fusion), kind=kCustom, calls=%fused_computation.1 | custom fusion | bytes 792576 | tf_op jit(solution)/shard_map/gather | solution.py:64
  264.7 1.0 broadcast_select_fusion
  265.7 10.5 %all-to-all-start.1 = ((bf16[32,48,128]{2,1,0:T(8,128)(2,1)}), bf16[32,48,128]{2,1,0:T(8,128)(2,1)S(1)}, u32[]{:S(2)}, u32[]{:S(2)}) async-start(bf16[32,48,128]{2,1,0:T(8,128)(2,1)} %broadcast_select_fusion), calls=%async_computation.1 | async-start | bytes 786432 | tf_op jit(solution)/shard_map/all_to_all | solution.py:66
  276.3 0.1 convert_reduce_fusion.1
  276.5 0.1 lt.135
  276.6 0.1 fusion.20
  276.7 12.6 %gather_fusion.2 = s32[1536]{0:T(1024)S(1)} fusion(s32[32,1024]{1,0:T(8,128)S(1)} %copy-done.1, s32[1536]{0:T(1024)S(1)} %reshape.250), kind=kCustom, calls=%fused_computation.2 | custom fusion | bytes 24576 | tf_op jit(solution)/shard_map/jit(take_along_axis)/gather | solution.py:36
  289.4 0.1 add.130
  289.6 1.0 fusion.2
  (28 shorter events, 0.5 us)
Async XLA Ops:
  6.5 176.8 %copy-start = (bf16[1,256,2048]{2,1,0:T(8,128)(2,1)S(1)}, bf16[1,256,2048]{2,1,0:T(8,128)(2,1)}, u32[]{:S(2)}) copy-start(bf16[1,256,2048]{2,1,0:T(8,128)(2,1)} %param.13) | copy-start | bytes 3145732
  6.5 19.7 %copy-start.1 = (s32[32,1024]{1,0:T(8,128)S(1)}, s32[32,1024]{1,0:T(8,128)}, u32[]{:S(2)}) copy-start(s32[32,1024]{1,0:T(8,128)} %param.9) | copy-start | bytes 393220
  6.5 65.7 %all-gather.2.cloned.1.call-start = ((), (), s32[]{:S(2)}) async-start(), calls=%async_computation.3 | async-start | bytes 2359296 | tf_op jit(solution)/shard_map/all_gather | solution.py:13
  26.2 234.0 %reduce-scatter.4.cloned.1.call-start = ((), (), s32[]{:S(2)}) async-start(), calls=%async_computation.4 | async-start | bytes 4456448
  77.7 103.3 %copy-start.4 = (bf16[1,2048,256]{2,1,0:T(8,128)(2,1)S(1)}, bf16[1,2048,256]{2,1,0:T(8,128)(2,1)}, u32[]{:S(2)}) copy-start(bf16[1,2048,256]{2,1,0:T(8,128)(2,1)} %param.11) | copy-start | bytes 3145732
  179.1 2.0 copy-start.2
  181.0 2.3 copy-start.5
  198.6 62.7 %copy-start.3 = (f32[1,1024]{1,0:T(1,128)S(1)}, f32[1,1024]{1,0:T(1,128)}, u32[]{:S(2)}) copy-start(f32[1,1024]{1,0:T(1,128)} %param.10) | copy-start | bytes 12292
  265.7 23.9 %all-to-all-start.1 = ((bf16[32,48,128]{2,1,0:T(8,128)(2,1)}), bf16[32,48,128]{2,1,0:T(8,128)(2,1)S(1)}, u32[]{:S(2)}, u32[]{:S(2)}) async-start(bf16[32,48,128]{2,1,0:T(8,128)(2,1)} %broadcast_select_fusion), calls=%async_computation.1 | async-start | bytes 786432 | tf_op jit(solution)/shard_map/all_to_all | solution.py:66
Sparse Core Ops, SparseCore 0:
  26.3 45.9 all-gather.1
  198.7 61.3 reduce-scatter.3
